TPU v7x, 256 devices: a 4x2x16 block of a 4x16x16 slice. The times are simulated.
256 devices in a mesh: grp: 2 (over y), ep: 32 (over z, core), tp: 4 (over x).
Axes of the slice: x: 4, y: 2, z: 16, core: 2. Of those that a mesh axis runs over, the one named last changes fastest.
The devices are a block of a 4x16x16 slice.
Arguments:
- outer_gate: bfloat16 [32768, 1024], P(('grp', 'ep'), 'tp'), parts along dimension 0, may hold values from -6 to 6
- inner_gate: bfloat16 [32768, 1024], P(('grp', 'ep'), 'tp'), parts along dimension 0, may hold values from -6 to 6
- conv_input: bfloat16 [32768, 1024], P(('grp', 'ep'), 'tp'), parts along dimension 0, may hold values from -6 to 6
- conv_taps: float32 [3, 1024], P(None, 'tp'), may hold values from -3.5 to 3.5
- mixer_weight: bfloat16 [1024, 2048], P('tp'), may hold values from -0.1875 to 0.1875
- expert_input: bfloat16 [32768, 2048], P(('grp', 'ep', 'tp')), parts along dimension 0, may hold values from -6 to 6
- norm_gain: float32 [2048], replicated, may hold values from 0.1 to 1.9
- expert_ids: int32 [32768, 2], P(('grp', 'ep', 'tp')), parts along dimension 0, may hold values from 0 to 31, all different within a row; in each aligned block of 128 rows (0 to 127, 128 to 255, ...) at most 10 rows name the same one
- route_weight: float32 [32768, 2], P(('grp', 'ep', 'tp')), parts along dimension 0, may hold values from 0.25 to 1
- gate_weight: bfloat16 [32, 2048, 3072], P('ep', None, 'tp'), may hold values from -0.125 to 0.125
- up_weight: bfloat16 [32, 2048, 3072], P('ep', None, 'tp'), may hold values from -0.125 to 0.125
- down_weight: bfloat16 [32, 3072, 2048], P('ep', 'tp'), may hold values from -0.109375 to 0.109375
Outputs:
- mixer_output: bfloat16 [32768, 2048], P(('grp', 'ep', 'tp')), parts along dimension 0
- expert_output: bfloat16 [32768, 2048], P(('grp', 'ep', 'tp')), parts along dimension 0
There are 2 independent parts, one for each index of `grp`. A program takes and returns all parts, laid end to end along the dimension named above; an argument that names none is the same for every part. Nothing has to cross between parts.
Inputs may be any that keep to these rules, and one draw needn't show every extreme that they name: `expert_ids`: each row names 2 different experts. Among the rows of one device no expert is named more than 10 times, a bound that some block reaches.
All inputs are finite; a program needn't handle non-finite values.
Results may differ from a plain program's by a relative error of at most 0.011.
Values may be sent and summed in bfloat16 or wider, within the bound.
A program may use at most 128 MiB of HBM per device.

v0:
```python
import jax
import jax.numpy as jnp
from jax import lax
from jax.sharding import Mesh
from jax.sharding import PartitionSpec as P

TAPS = 3
EP = ("ep_0", "ep_1")
GRP_EP = ("grp", "ep_0", "ep_1")
GRP_EP_TP = ("grp", "ep_0", "ep_1", "tp")


epsilon = 1e-06


def shifted(value, axis, steps):
    count = lax.axis_size(axis)
    initial, last = (max(0, -steps), min(count, count - steps))
    return lax.ppermute(value, axis, [(source, source + steps) for source in range(initial, last)])


def split_up(value, dim, peers):
    lengths = value.shape
    tiles = value.reshape(*lengths[:dim], peers, lengths[dim] // peers, *lengths[dim + 1 :])
    return jnp.moveaxis(tiles, dim, 0)


def summed_on_arrival(value, axis, dim):
    tiles = split_up(value, dim, lax.axis_size(axis))
    arrived = lax.all_to_all(tiles, axis, split_axis=0, concat_axis=0, tiled=True)
    return arrived.astype(jnp.float32).sum(axis=0)


def laid_out(tiles, dim):
    tiles = jnp.moveaxis(tiles, 0, dim)
    lengths = tiles.shape
    return tiles.reshape(*lengths[:dim], lengths[dim] * lengths[dim + 1], *lengths[dim + 2 :])


def exchange_in_order(tiles, axes, order):
    lengths = [lax.axis_size(a) for a in axes]
    tiles = tiles.reshape(*lengths, *tiles.shape[1:])
    for k in order:
        tiles = lax.all_to_all(tiles, axes[k], split_axis=k, concat_axis=k, tiled=True)
    return tiles.reshape(-1, *tiles.shape[len(axes) :])


def two_step_exchange(value, groups, order, split_dim, concat_dim):
    peers = lax.axis_size(groups[0]) * lax.axis_size(groups[1])
    tiles = split_up(value, split_dim, peers)
    return laid_out(exchange_in_order(tiles, groups, order), concat_dim)


def on_device(
    outer_gate,
    inner_gate,
    conv_input,
    conv_taps,
    mixer_weight,
    expert_input,
    norm_gain,
    expert_ids,
    route_weight,
    gate_weight,
    up_weight,
    down_weight,
):
    gated_rows = inner_gate.astype(jnp.float32) * conv_input.astype(jnp.float32)
    length = gated_rows.shape[0]
    earlier = shifted(gated_rows[length - (TAPS - 1) :], EP, 1)
    padded = jnp.concatenate([earlier, gated_rows], axis=0)
    convolved = jnp.zeros_like(gated_rows)
    for tap_index in range(TAPS):
        convolved = convolved + conv_taps[tap_index] * padded[tap_index : tap_index + length]
    mixed = (outer_gate.astype(jnp.float32) * convolved).astype(jnp.bfloat16)
    mixer_output = summed_on_arrival(
        jnp.dot(mixed, mixer_weight, preferred_element_type=jnp.float32).astype(jnp.bfloat16),
        "tp",
        0,
    ).astype(jnp.bfloat16)
    inputs = expert_input.astype(jnp.float32)
    normed = (
        inputs * lax.rsqrt(jnp.mean(inputs * inputs, axis=1, keepdims=True) + epsilon) * norm_gain
    ).astype(jnp.bfloat16)
    tokens_here, top_count = expert_ids.shape
    model_width = expert_input.shape[1]
    expert_count = lax.axis_size(EP) * gate_weight.shape[0]
    capacity = 5 * tokens_here * top_count // (4 * expert_count)
    flat_ids = expert_ids.reshape(-1)
    one_hot = (flat_ids[:, None] == jnp.arange(expert_count, dtype=jnp.int32)[None, :]).astype(
        jnp.int32
    )
    ranks = jnp.sum((jnp.cumsum(one_hot, axis=0) - 1) * one_hot, axis=1)
    target = flat_ids * capacity + ranks
    duplicates = jnp.broadcast_to(
        normed[:, None, :], (tokens_here, top_count, model_width)
    ).reshape(-1, model_width)
    outgoing = (
        jnp.zeros((expert_count * capacity, model_width), jnp.bfloat16).at[target].set(duplicates)
    )
    gate_local = gate_weight[0]
    up_local = up_weight[0]
    down_local = down_weight[0]
    arrived = two_step_exchange(
        outgoing.reshape(expert_count, capacity, model_width), ("ep_0", "ep_1"), (1, 0), 0, 0
    )
    sources = arrived.shape[0]
    slot_count = arrived.shape[1]
    stacked = arrived.reshape(sources * slot_count, model_width)
    block_rows = lax.all_gather(stacked, "tp", axis=0, tiled=True)
    gate_value = jnp.dot(block_rows, gate_local, preferred_element_type=jnp.float32)
    up_value = jnp.dot(block_rows, up_local, preferred_element_type=jnp.float32)
    hidden = (jax.nn.silu(gate_value) * up_value).astype(jnp.bfloat16)
    own_sums = summed_on_arrival(
        jnp.dot(hidden, down_local, preferred_element_type=jnp.float32).astype(jnp.bfloat16),
        "tp",
        0,
    ).astype(jnp.bfloat16)
    answers = two_step_exchange(
        own_sums.reshape(sources, slot_count, model_width), ("ep_0", "ep_1"), (1, 0), 0, 0
    )
    picked = answers.reshape(expert_count * capacity, model_width)[target]
    picked = picked.astype(jnp.float32).reshape(tokens_here, top_count, model_width)
    expert_output = jnp.sum(picked * route_weight[:, :, None], axis=1).astype(jnp.bfloat16)
    return (mixer_output, expert_output)


def solution(mesh):
    finer = Mesh(
        mesh.devices.reshape(mesh.shape["grp"], 16, 2, mesh.shape["tp"]),
        ("grp", "ep_0", "ep_1", "tp"),
    )
    placed = (
        P(GRP_EP, "tp"),
        P(GRP_EP, "tp"),
        P(GRP_EP, "tp"),
        P(None, "tp"),
        P("tp", None),
        P(GRP_EP_TP, None),
        P(),
        P(GRP_EP_TP, None),
        P(GRP_EP_TP, None),
        P(EP, None, "tp"),
        P(EP, None, "tp"),
        P(EP, "tp", None),
    )
    return jax.shard_map(
        on_device,
        mesh=finer,
        in_specs=placed,
        out_specs=(P(GRP_EP_TP, None), P(GRP_EP_TP, None)),
        check_vma=False,
    )
```

profile of v0, /device:TPU:33, one launch (start us, length us, event | category | flops | bytes accessed | tf_op | source)
XLA Modules:
  0.0 406.3 jit_solution(17758050569771702696)
XLA Ops:
  12.7 1.7 broadcast_in_dim.5
  14.4 2.3 reshape.93
  16.8 4.0 scatter_custom_fusion
  20.7 3.3 reshape_reshape_reshape.12
  24.1 2.3 copy.24
  26.4 24.8 %all_to_all.30 = bf16[16,2,1,10,2048]{4,0,3,2,1:T(8,128)(2,1)S(1)} all-to-all(bf16[16,2,1,10,2048]{4,0,3,2,1:T(8,128)(2,1)S(1)} %copy.24), channel_id=1, replica_groups=mesh['grp'=2,'ep_0'=16,'ep_1'=2,'tp'=4] {'ep_1'}, dimensions={1} | all-to-all | bytes 2621440 | tf_op jit(solution)/shard_map/all_to_all | solution.py:44
  51.2 1.3 copy.25
  52.6 62.6 %all_to_all.31 = bf16[16,2,1,10,2048]{4,1,3,2,0:T(2,128)(2,1)S(1)} all-to-all(bf16[16,2,1,10,2048]{4,1,3,2,0:T(2,128)(2,1)S(1)} %copy.25), channel_id=1, replica_groups=mesh['grp'=2,'ep_0'=16,'ep_1'=2,'tp'=4] {'ep_0'}, dimensions={0} | all-to-all | bytes 2621440 | tf_op jit(solution)/shard_map/all_to_all | solution.py:44
  115.1 2.0 copy.26
  117.1 3.6 reshape_reshape_reshape.13
  120.8 64.2 %all-gather.2.cloned.1.call-done = bf16[1280,2048]{1,0:T(8,128)(2,1)} async-done(((bf16[320,2048]{1,0:T(8,128)(2,1)}), bf16[1280,2048]{1,0:T(8,128)(2,1)}) %all-gather.2.cloned.1.call-update) | async-done | bytes 5242896 | tf_op jit(solution)/shard_map/all_gather | solution.py:110
  185.0 7.2 %fusion.3 = f32[1280,768]{1,0:T(8,128)S(1)} fusion(bf16[1280,2048]{1,0:T(8,128)(2,1)} %all-gather.2.cloned.1.call-done, bf16[1,2048,768]{2,1,0:T(8,128)(2,1)} %param.21), kind=kOutput, calls=%fused_computation.7 | convolution fusion | flops 4026531840 | bytes 12320768 | tf_op jit(solution)/shard_map/dot_general | solution.py:111
  192.2 4.8 %fusion = bf16[1280,768]{1,0:T(8,128)(2,1)S(1)} fusion(bf16[1280,2048]{1,0:T(8,128)(2,1)S(1)} %copy-done.8, f32[1280,768]{1,0:T(8,128)S(1)} %fusion.3, bf16[1,2048,768]{2,1,0:T(8,128)(2,1)S(1)} %copy-done.9), kind=kOutput, calls=%fused_computation.4 | convolution fusion | flops 4032430080 | bytes 14286848 | tf_op jit(solution)/shard_map/dot_general | solution.py:112
  197.0 6.1 %convolution_convert_fusion = bf16[1280,2048]{1,0:T(8,128)(2,1)} fusion(bf16[1280,768]{1,0:T(8,128)(2,1)S(1)} %fusion, bf16[1,768,2048]{2,1,0:T(8,128)(2,1)S(1)} %copy-done), kind=kOutput, calls=%fused_computation.2 | convolution fusion | flops 4029153280 | bytes 10354688 | tf_op jit(solution)/shard_map/dot_general | solution.py:115
  203.1 5.3 %all-to-all-start.3 = ((bf16[4,320,2048]{2,1,0:T(8,128)(2,1)}), bf16[4,320,2048]{2,1,0:T(8,128)(2,1)}, u32[]{:S(2)}, u32[]{:S(2)}) async-start(bf16[4,320,2048]{2,1,0:T(8,128)(2,1)} %bitcast.39), calls=%async_computation.3 | async-start | bytes 10485760 | tf_op jit(solution)/shard_map/all_to_all | solution.py:30
  208.5 3.9 collective-permute-start
  213.1 2.1 convolution_convert_fusion.1
  215.2 52.4 %all-to-all-done.3 = bf16[4,320,2048]{2,1,0:T(8,128)(2,1)} async-done(((bf16[4,320,2048]{2,1,0:T(8,128)(2,1)}), bf16[4,320,2048]{2,1,0:T(8,128)(2,1)}, u32[]{:S(2)}, u32[]{:S(2)}) %all-to-all-start.3) | async-done | bytes 5242912 | tf_op jit(solution)/shard_map/all_to_all | solution.py:30
  267.7 5.0 %reduce_sum.57 = bf16[320,2048]{1,0:T(8,128)(2,1)} reduce(bf16[4,320,2048]{2,1,0:T(8,128)(2,1)} %all-to-all-done.3, bf16[]{:T(256)} %constant.9.clone.1), dimensions={0}, to_apply=%region_6.7 | reduce | flops 1966080 | bytes 6553602 | tf_op jit(solution)/shard_map/reduce_sum | solution.py:31
  272.7 2.3 reshape_reshape_reshape.14
  275.7 7.0 %all_to_all.32 = bf16[16,2,1,10,2048]{4,0,3,2,1:T(8,128)(2,1)} all-to-all(bf16[16,2,1,10,2048]{4,0,3,2,1:T(8,128)(2,1)S(1)} %copy.27), channel_id=1, replica_groups=mesh['grp'=2,'ep_0'=16,'ep_1'=2,'tp'=4] {'ep_1'}, dimensions={1} | all-to-all | bytes 2621440 | tf_op jit(solution)/shard_map/all_to_all | solution.py:44
  282.7 3.9 all-to-all-start
  286.6 3.7 copy.28
  290.4 22.2 %all-to-all-done = bf16[4,128,2048]{2,1,0:T(8,128)(2,1)S(1)} async-done(((bf16[4,128,2048]{2,1,0:T(8,128)(2,1)}), bf16[4,128,2048]{2,1,0:T(8,128)(2,1)S(1)}, u32[]{:S(2)}, u32[]{:S(2)}) %all-to-all-start) | async-done | bytes 2097184 | tf_op jit(solution)/shard_map/all_to_all | solution.py:30
  312.6 12.1 %all-to-all-start.5 = ((bf16[16,2,1,10,2048]{4,1,3,2,0:T(2,128)(2,1)}), bf16[16,2,1,10,2048]{4,1,3,2,0:T(2,128)(2,1)}, u32[]{:S(2)}, u32[]{:S(2)}) async-start(bf16[16,2,1,10,2048]{4,1,3,2,0:T(2,128)(2,1)} %copy.28), calls=%async_computation.5 | async-start | bytes 2621440 | tf_op jit(solution)/shard_map/all_to_all | solution.py:44
  324.8 1.3 reduce_sum.53
  326.1 56.1 %all-to-all-done.5 = bf16[16,2,1,10,2048]{4,1,3,2,0:T(2,128)(2,1)} async-done(((bf16[16,2,1,10,2048]{4,1,3,2,0:T(2,128)(2,1)}), bf16[16,2,1,10,2048]{4,1,3,2,0:T(2,128)(2,1)}, u32[]{:S(2)}, u32[]{:S(2)}) %all-to-all-start.5) | async-done | bytes 1310752 | tf_op jit(solution)/shard_map/all_to_all | solution.py:44
  382.2 2.0 copy.29
  384.1 1.3 reshape_reshape_reshape.15
  385.5 5.0 %gather_fusion = bf16[256,2048]{1,0:T(8,128)(2,1)} fusion(bf16[320,2048]{1,0:T(8,128)(2,1)} %reshape_reshape_reshape.15, s32[1024]{0:T(1024)S(1)} %pad_clamp_fusion), kind=kCustom, calls=%fused_computation | custom fusion | bytes 2098176 | tf_op jit(solution)/shard_map/gather | solution.py:122
  390.4 3.4 reshape.80
  393.8 5.6 %multiply_reduce_fusion = bf16[128,2048]{1,0:T(8,128)(2,1)} fusion(f32[128,2,2048]{2,1,0:T(2,128)} %reshape.80, f32[128,2]{1,0:T(8,128)S(1)} %copy.30), kind=kLoop, calls=%fused_computation.10 | loop fusion | flops 786432 | bytes 2622464 | tf_op jit(solution)/shard_map/reduce_sum | solution.py:124
  (45 shorter events, 7.3 us)
Async XLA Ops:
  7.2 189.9 %copy-start = (bf16[1,768,2048]{2,1,0:T(8,128)(2,1)S(1)}, bf16[1,768,2048]{2,1,0:T(8,128)(2,1)}, u32[]{:S(2)}) copy-start(bf16[1,768,2048]{2,1,0:T(8,128)(2,1)} %param.23) | copy-start | bytes 9437188
  7.2 177.8 %all-gather.2.cloned.1.call-start = ((), (), s32[]{:S(2)}) async-start(), calls=%async_computation.6 | async-start | bytes 6553600 | tf_op jit(solution)/shard_map/all_gather | solution.py:110
  184.9 7.3 %copy-start.8 = (bf16[1280,2048]{1,0:T(8,128)(2,1)S(1)}, bf16[1280,2048]{1,0:T(8,128)(2,1)}, u32[]{:S(2)}) copy-start(bf16[1280,2048]{1,0:T(8,128)(2,1)} %all-gather.2.cloned.1.call-done) | copy-start | bytes 15728644
  185.0 7.3 %copy-start.9 = (bf16[1,2048,768]{2,1,0:T(8,128)(2,1)S(1)}, bf16[1,2048,768]{2,1,0:T(8,128)(2,1)}, u32[]{:S(2)}) copy-start(bf16[1,2048,768]{2,1,0:T(8,128)(2,1)} %param.22) | copy-start | bytes 9437188
  203.1 5.3 %copy-start.4 = (bf16[512,256]{1,0:T(8,128)(2,1)S(1)}, bf16[512,256]{1,0:T(8,128)(2,1)}, u32[]{:S(2)}) copy-start(bf16[512,256]{1,0:T(8,128)(2,1)} %param.14) | copy-start | bytes 786436
  203.1 5.3 %copy-start.5 = (bf16[512,256]{1,0:T(8,128)(2,1)S(1)}, bf16[512,256]{1,0:T(8,128)(2,1)}, u32[]{:S(2)}) copy-start(bf16[512,256]{1,0:T(8,128)(2,1)} %param.13) | copy-start | bytes 786436
  203.1 9.3 %copy-start.6 = (f32[3,256]{1,0:T(4,128)S(1)}, f32[3,256]{1,0:T(4,128)}, u32[]{:S(2)}) copy-start(f32[3,256]{1,0:T(4,128)} %param.15) | copy-start | bytes 9220
  203.1 10.0 %copy-start.2 = (bf16[256,2048]{1,0:T(8,128)(2,1)S(1)}, bf16[256,2048]{1,0:T(8,128)(2,1)}, u32[]{:S(2)}) copy-start(bf16[256,2048]{1,0:T(8,128)(2,1)} %param.16) | copy-start | bytes 3145732
  203.1 10.0 %copy-start.3 = (bf16[512,256]{1,0:T(8,128)(2,1)S(1)}, bf16[512,256]{1,0:T(8,128)(2,1)}, u32[]{:S(2)}) copy-start(bf16[512,256]{1,0:T(8,128)(2,1)} %param.12) | copy-start | bytes 786436
  203.1 64.6 %all-to-all-start.3 = ((bf16[4,320,2048]{2,1,0:T(8,128)(2,1)}), bf16[4,320,2048]{2,1,0:T(8,128)(2,1)}, u32[]{:S(2)}, u32[]{:S(2)}) async-start(bf16[4,320,2048]{2,1,0:T(8,128)(2,1)} %bitcast.39), calls=%async_computation.3 | async-start | bytes 10485760 | tf_op jit(solution)/shard_map/all_to_all | solution.py:30
  208.5 4.6 %collective-permute-start = (f32[2,256]{1,0:T(2,128)S(1)}, f32[2,256]{1,0:T(2,128)S(1)}, u32[]{:S(2)}, u32[]{:S(2)}) collective-permute-start(f32[2,256]{1,0:T(2,128)S(1)} %slice.34), channel_id=1, source_target_pairs={{0,4},{4,8},{8,12},{12,16},{16,20},{20,24},{24,28},{28,32},{32,36}... | collective-permute-start | bytes 6152 | tf_op jit(solution)/shard_map/ppermute | solution.py:19
  282.7 29.9 %all-to-all-start = ((bf16[4,128,2048]{2,1,0:T(8,128)(2,1)}), bf16[4,128,2048]{2,1,0:T(8,128)(2,1)S(1)}, u32[]{:S(2)}, u32[]{:S(2)}) async-start(bf16[4,128,2048]{2,1,0:T(8,128)(2,1)} %bitcast.3), calls=%async_computation | async-start | bytes 4194304 | tf_op jit(solution)/shard_map/all_to_all | solution.py:30
  286.6 38.1 %copy-start.7 = (f32[128,2]{0,1:T(2,128)S(1)}, f32[128,2]{0,1:T(2,128)}, u32[]{:S(2)}) copy-start(f32[128,2]{0,1:T(2,128)} %param.20) | copy-start | bytes 3076
  312.6 69.6 %all-to-all-start.5 = ((bf16[16,2,1,10,2048]{4,1,3,2,0:T(2,128)(2,1)}), bf16[16,2,1,10,2048]{4,1,3,2,0:T(2,128)(2,1)}, u32[]{:S(2)}, u32[]{:S(2)}) async-start(bf16[16,2,1,10,2048]{4,1,3,2,0:T(2,128)(2,1)} %copy.28), calls=%async_computation.5 | async-start | bytes 2621440 | tf_op jit(solution)/shard_map/all_to_all | solution.py:44
  385.5 14.0 %copy-start.1 = (bf16[1,768,2048]{2,1,0:T(8,128)(2,1)S(1)}, bf16[1,768,2048]{2,1,0:T(8,128)(2,1)}, u32[]{:S(2)}) copy-start(bf16[1,768,2048]{2,1,0:T(8,128)(2,1)} %param.23) | copy-start | bytes 9437188
Sparse Core Ops, SparseCore 0:
  120.9 64.0 all-gather.1
where the time goes:
time: 412 us; the launch traced here: 406 us
  waiting for transfers between devices  196 us (48%)
  blocking collectives  94.4 us (23%)
  local copies, waits for them, and re-layouts  40.7 us (10%)
  starting transfers between devices  25.3 us (6%)
  matrix products  20.2 us (5%)
  other arithmetic  15.8 us (4%)
  between operations  14.3 us (3%)
    all_to_all x3, blocking collectives, exchange_in_order(): lax.all_to_all(tiles, axes[k], split_axis=k, concat_axis=k, tiled=True)  94.4 us
    all_to_all x2, waiting for transfers between devices, summed_on_arrival(): lax.all_to_all(tiles, axis, split_axis=0, concat_axis=0, tiled=True)  74.7 us
    all_gather x1, waiting for transfers between devices, on_device(): block_rows = lax.all_gather(stacked, 'tp', axis=0, tiled=True)  64.2 us
    all_to_all x1, waiting for transfers between devices, exchange_in_order(): lax.all_to_all(tiles, axes[k], split_axis=k, concat_axis=k, tiled=True)  56.1 us
    all_to_all x1, starting transfers between devices, exchange_in_order(): lax.all_to_all(tiles, axes[k], split_axis=k, concat_axis=k, tiled=True)  12.1 us
    all_to_all x2, starting transfers between devices, summed_on_arrival(): lax.all_to_all(tiles, axis, split_axis=0, concat_axis=0, tiled=True)  9.19 us
    all_to_all x4, local copies, waits for them, and re-layouts, exchange_in_order(): lax.all_to_all(tiles, axes[k], split_axis=k, concat_axis=k, tiled=True)  9.04 us
    another operation x4, local copies, waits for them, and re-layouts, exchange_in_order(): tiles = tiles.reshape(*lengths, *tiles.shape[1:])  8.68 us
  transfers between devices with their start and end apart: 5, of which 5 were waited for; matrix products, arithmetic and copies ran while one was open for 2% of the time, Pallas kernels for 0%

commit v1 on v0

v1 whole, which is shorter than its diff:
```python
import functools

import jax
import jax.numpy as jnp
from jax import lax
from jax.experimental import pallas as pl
from jax.experimental.pallas import tpu as pltpu
from jax.sharding import PartitionSpec as P

TAPS = 3
CORES = 2
LANES = 128
EPSILON = 1e-06
MESH = pl.DeviceIdType.MESH
F32 = jnp.float32
BF16 = jnp.bfloat16


def remote(source, target, send, recv, where):
    return pltpu.make_async_remote_copy(
        src_ref=source,
        dst_ref=target,
        send_sem=send,
        recv_sem=recv,
        device_id=where,
        device_id_type=MESH,
    )


def dot(a, b):
    return jnp.dot(a, b, preferred_element_type=F32)


def kernel(
    n_ep,
    n_tp,
    cap,
    ids_ref,
    route_ref,
    tokens_ref,
    gain_ref,
    taps_ref,
    outer_hbm,
    inner_hbm,
    conv_hbm,
    mixw_hbm,
    gate_hbm,
    up_hbm,
    down_hbm,
    mixer_ref,
    expert_ref,
    outer,
    inner,
    conv,
    mixw,
    gate_w,
    up_w,
    down_w,
    normed,
    picks,
    wide,
    outgoing,
    gathered,
    rows_f,
    rows_b,
    hidden,
    partial,
    first_in,
    second_in,
    combined,
    summed,
    returned,
    answers,
    tail_out,
    tail_in,
    gated,
    mix_partial,
    mix_first,
    mix_second,
    mix_combined,
    load_sem,
    halo_send,
    halo_recv,
    z_send,
    z_recv,
    gather_send,
    gather_recv,
    relay_send,
    relay_recv,
    first_send,
    first_recv,
    direct_send,
    comb_send,
    second_recv,
    back_send,
    back_recv,
    mix_send,
    mix_first_recv,
    mix_second_recv,
):
    n_z = n_ep // CORES
    groups = n_z // 2
    last = groups - 1
    count = 2 * n_z
    tokens, width = tokens_ref.shape
    strips = width // LANES
    chunk = cap * strips
    slots = picks.shape[0]
    used = count * cap
    batch = 4 * 2 * CORES * cap

    me = lax.axis_index("ep")
    x = lax.axis_index("tp")
    z = me // CORES
    core = me % CORES
    right = {"tp": (x + 1) % n_tp}
    left = {"tp": (x + n_tp - 1) % n_tp}

    barrier = pltpu.get_barrier_semaphore()

    @pl.loop(1, n_ep)
    def _(k):
        pl.semaphore_signal(
            barrier, inc=1, device_id={"ep": (me + k) % n_ep}, device_id_type=MESH
        )

    pl.semaphore_signal(barrier, inc=1, device_id=right, device_id_type=MESH)
    pl.semaphore_signal(barrier, inc=1, device_id=left, device_id_type=MESH)

    loads = [
        pltpu.make_async_copy(source, target, load_sem.at[k])
        for k, (source, target) in enumerate(
            (
                (inner_hbm, inner),
                (conv_hbm, conv),
                (outer_hbm, outer),
                (mixw_hbm, mixw),
                (gate_hbm, gate_w),
                (up_hbm, up_w),
                (down_hbm, down_w),
            )
        )
    ]
    for load in loads:
        load.start()

    row = lax.broadcasted_iota(jnp.int32, (slots, tokens), 0)
    place = row * 0
    for k in range(1, slots // cap + 1):
        place = place + (row >= k * cap).astype(jnp.int32)
    slot = row - place * cap
    group_of = lax.shift_right_logical(place, 2)
    half_of = lax.shift_right_logical(place, 1) & 1
    offset = jnp.where(
        half_of == 0, group_of + 1, jnp.where(group_of == last, 0, n_z - 1 - group_of)
    )
    target_z = z - offset
    target_z = jnp.where(target_z < 0, target_z + n_z, target_z)
    expert = jnp.where(row < used, target_z * CORES + (place & 1), -1)
    first_named = ids_ref[0:1, :] == expert
    second_named = ids_ref[1:2, :] == expert
    named = jnp.where(first_named, 1.0, 0.0) + jnp.where(second_named, 1.0, 0.0)
    before = lax.broadcasted_iota(jnp.int32, (tokens, tokens), 0) < lax.broadcasted_iota(
        jnp.int32, (tokens, tokens), 1
    )
    rank = dot(named.astype(BF16), jnp.where(before, 1.0, 0.0).astype(BF16))
    chosen = jnp.where(rank == slot.astype(F32), named, 0.0)
    weight = jnp.where(first_named, route_ref[0:1, :], 0.0) + jnp.where(
        second_named, route_ref[1:2, :], 0.0
    )
    picks[...] = chosen * weight

    values = tokens_ref[...].astype(F32)
    mean = jnp.mean(values * values, axis=1, keepdims=True)
    normed[...] = (values * lax.rsqrt(mean + EPSILON) * gain_ref[...]).astype(BF16)
    one_hot = chosen[0:used, :].astype(BF16)
    for pair in range(strips // 2):
        rows = dot(one_hot, normed[:, 2 * pair * LANES : 2 * (pair + 1) * LANES])
        wide[pl.ds(2 * pair, used, stride=strips), :] = rows[:, :LANES]
        wide[pl.ds(2 * pair + 1, used, stride=strips), :] = rows[:, LANES:]

    @pl.loop(0, count)
    def _(k):
        outgoing[k] = wide[pl.ds(pl.multiple_of(k * chunk, 16), chunk), :].astype(BF16)

    loads[0].wait()
    loads[1].wait()
    length = inner.shape[0]
    gated[pl.ds(8, length), :] = inner[...].astype(F32) * conv[...].astype(F32)
    tail_out[...] = gated[pl.ds(length, 8), :]

    pl.semaphore_wait(barrier, n_ep + 1)

    def sent(g, half, to_core, from_slot):
        offset = g + 1 if half == 0 else n_z - 1 - g
        return remote(
            outgoing.at[from_slot],
            gathered.at[g, 0, half, core],
            z_send.at[0],
            z_recv.at[g, half],
            {"ep": ((z + n_z - offset) % n_z) * CORES + to_core},
        )

    @pl.loop(0, last)
    def _(g):
        for half in range(2):
            for to_core in range(CORES):
                sent(g, half, to_core, 4 * g + 2 * half + to_core).start()

    for to_core in range(CORES):
        sent(last, 0, to_core, 4 * last + to_core).start()
    other = 1 - core
    partner = {"ep": z * CORES + other}
    remote(
        outgoing.at[4 * last + 2 + other],
        gathered.at[last, 0, 1, core],
        z_send.at[0],
        z_recv.at[last, 1],
        partner,
    ).start()
    gathered[last, 0, 1, core] = outgoing[4 * last + 2 + core]
    halo = remote(
        tail_out, tail_in, halo_send.at[0], halo_recv.at[0], {"ep": (me + 1) % n_ep}
    )
    halo.start()

    for load in loads[2:4]:
        load.wait()
    halo.wait()
    gated[0:8, :] = jnp.where(me > 0, tail_in[...], 0.0)
    convolved = jnp.zeros((length, inner.shape[1]), F32)
    for tap in range(TAPS):
        convolved = convolved + taps_ref[tap : tap + 1, :] * gated[
            pl.ds(8 - (TAPS - 1) + tap, length), :
        ]
    inner[...] = (outer[...].astype(F32) * convolved).astype(BF16)
    half_rows = tokens // 2

    @pl.loop(0, n_tp * 2)
    def _(k):
        owner = (x + k // 2) % n_tp
        start = pl.multiple_of(owner * tokens + (k % 2) * half_rows, 16)
        mixed = inner[pl.ds(start, half_rows), :]
        for part in range(width // 512):
            columns = slice(part * 512, (part + 1) * 512)
            mix_partial[k // 2, k % 2, :, columns] = dot(mixed, mixw[:, columns]).astype(BF16)

    for load in loads[4:]:
        load.wait()

    def gather(g):
        block = gathered.at[g, 0, 0]
        remote(block, block, z_send.at[0], z_recv.at[g, 0], right).wait_recv()

        @pl.when(g < last)
        def _():
            block = gathered.at[g, 0, 1]
            remote(block, block, z_send.at[0], z_recv.at[g, 1], right).wait_recv()

        @pl.when(g == last)
        def _():
            block = gathered.at[g, 0, 1, 0]
            remote(block, block, z_send.at[0], z_recv.at[g, 1], right).wait_recv()

        remote(
            gathered.at[g, 0], gathered.at[g, 3], gather_send.at[0], gather_recv.at[g, 0], right
        ).start()
        remote(
            gathered.at[g, 0], gathered.at[g, 1], gather_send.at[1], gather_recv.at[g, 1], left
        ).start()

    def relay(g):
        remote(
            gathered.at[g, 0], gathered.at[g, 3], gather_send.at[0], gather_recv.at[g, 0], right
        ).wait_recv()
        remote(
            gathered.at[g, 3, 0], gathered.at[g, 2, 0], relay_send.at[0], relay_recv.at[g, 0], right
        ).start()
        remote(
            gathered.at[g, 0], gathered.at[g, 1], gather_send.at[1], gather_recv.at[g, 1], left
        ).wait_recv()
        remote(
            gathered.at[g, 1, 1], gathered.at[g, 2, 1], relay_send.at[1], relay_recv.at[g, 1], left
        ).start()

    def compute(g):
        remote(
            gathered.at[g, 3, 0], gathered.at[g, 2, 0], relay_send.at[0], relay_recv.at[g, 0], right
        ).wait_recv()
        remote(
            gathered.at[g, 1, 1], gathered.at[g, 2, 1], relay_send.at[1], relay_recv.at[g, 1], left
        ).wait_recv()
        for k in range(batch // cap):
            rows_f[k * chunk : (k + 1) * chunk, :] = gathered[
                g, k // 4, (k // 2) % 2, k % 2
            ].astype(F32)
        for strip in range(strips):
            rows_b[:, strip * LANES : (strip + 1) * LANES] = rows_f[
                pl.ds(strip, batch, stride=strips), :
            ].astype(BF16)
        units = hidden.shape[1]
        step = min(256, units)
        for part in range(units // step):
            columns = slice(part * step, (part + 1) * step)
            gate = dot(rows_b[...], gate_w[:, columns])
            up = dot(rows_b[...], up_w[:, columns])
            hidden[:, columns] = (gate / (1.0 + jnp.exp(-gate)) * up).astype(BF16)
        for pair in range(strips // 2):
            rows = dot(hidden[...], down_w[:, 2 * pair * LANES : 2 * (pair + 1) * LANES])
            rows_f[pl.ds(2 * pair, batch, stride=strips), :] = rows[:, :LANES]
            rows_f[pl.ds(2 * pair + 1, batch, stride=strips), :] = rows[:, LANES:]
        for k in range(batch // cap):
            partial[g, k // 4, (k // 2) % 2, k % 2] = rows_f[
                k * chunk : (k + 1) * chunk, :
            ].astype(BF16)
        remote(
            partial.at[g, 2, 0], first_in.at[g, 0], first_send.at[0], first_recv.at[g, 0], right
        ).start()
        remote(
            partial.at[g, 2, 1], first_in.at[g, 1], first_send.at[1], first_recv.at[g, 1], left
        ).start()
        remote(
            partial.at[g, 1, 1], second_in.at[g, 0, 1], direct_send.at[0], second_recv.at[g, 0], right
        ).start()
        remote(
            partial.at[g, 3, 0], second_in.at[g, 1, 0], direct_send.at[1], second_recv.at[g, 1], left
        ).start()

    def combine(g):
        for side, slot, where in ((0, 1, right), (1, 3, left)):
            remote(
                partial.at[g, 2, side], first_in.at[g, side], first_send.at[side],
                first_recv.at[g, side], where,
            ).wait_recv()
            combined[g, side] = (
                partial[g, slot, side].astype(F32) + first_in[g, side].astype(F32)
            ).astype(BF16)
            remote(
                combined.at[g, side], second_in.at[g, side, side], comb_send.at[side],
                second_recv.at[g, side], where,
            ).start()

    def back(g, half, to_core):
        offset = g + 1 if half == 0 else n_z - 1 - g
        return remote(
            summed.at[4 * g + 2 * half + to_core],
            returned.at[g, half, core],
            back_send.at[0],
            back_recv.at[g, half],
            {"ep": ((z + offset) % n_z) * CORES + to_core},
        )

    def give_back(g):
        for side, where in ((0, right), (1, left)):
            block = second_in.at[g, side]
            remote(block, block, comb_send.at[side], second_recv.at[g, side], where).wait_recv()
        for half in range(2):
            for from_core in range(CORES):
                summed[4 * g + 2 * half + from_core] = (
                    partial[g, 0, half, from_core].astype(F32)
                    + second_in[g, 0, half, from_core].astype(F32)
                    + second_in[g, 1, half, from_core].astype(F32)
                ).astype(BF16)

        @pl.when(g < last)
        def _():
            for half in range(2):
                for to_core in range(CORES):
                    back(g, half, to_core).start()

        @pl.when(g == last)
        def _():
            for to_core in range(CORES):
                back(last, 0, to_core).start()
            remote(
                summed.at[4 * last + 2 + other],
                returned.at[last, 1, core],
                back_send.at[0],
                back_recv.at[last, 1],
                partner,
            ).start()
            returned[last, 1, core] = summed[4 * last + 2 + core]

    def mix_start():
        remote(
            mix_partial.at[2, 0], mix_first.at[0], mix_send.at[0], mix_first_recv.at[0], right
        ).start()
        remote(
            mix_partial.at[2, 1], mix_first.at[1], mix_send.at[1], mix_first_recv.at[1], left
        ).start()
        remote(
            mix_partial.at[1, 1], mix_second.at[0, 1], mix_send.at[2], mix_second_recv.at[0, 1], right
        ).start()
        remote(
            mix_partial.at[3, 0], mix_second.at[1, 0], mix_send.at[3], mix_second_recv.at[1, 0], left
        ).start()

    def mix_combine():
        for side, slot, where in ((0, 1, right), (1, 3, left)):
            remote(
                mix_partial.at[2, side], mix_first.at[side], mix_send.at[side],
                mix_first_recv.at[side], where,
            ).wait_recv()
            mix_combined[side] = (
                mix_partial[slot, side].astype(F32) + mix_first[side].astype(F32)
            ).astype(BF16)
            remote(
                mix_combined.at[side], mix_second.at[side, side], mix_send.at[4 + side],
                mix_second_recv.at[side, side], where,
            ).start()

    @pl.loop(0, groups + 4)
    def _(t):
        @pl.when((t >= 2) & (t < groups + 2))
        def _():
            compute(t - 2)

        @pl.when((t >= 3) & (t < groups + 3))
        def _():
            combine(t - 3)

        @pl.when(t == groups + 2)
        def _():
            mix_start()

        @pl.when(t >= 4)
        def _():
            give_back(t - 4)

        @pl.when((t >= 1) & (t < groups + 1))
        def _():
            relay(t - 1)

        @pl.when(t < groups)
        def _():
            gather(t)

    mix_combine()
    for side in range(2):
        for half in range(2):
            block = mix_second.at[side, half]
            remote(
                block, block, mix_send.at[0], mix_second_recv.at[side, half], right
            ).wait_recv()
    for half in range(2):
        mixer_ref[half * half_rows : (half + 1) * half_rows, :] = (
            mix_partial[0, half].astype(F32)
            + mix_second[0, half].astype(F32)
            + mix_second[1, half].astype(F32)
        ).astype(BF16)

    for g in range(groups):
        for half in range(2):
            block = returned.at[g, half] if (g, half) != (last, 1) else returned.at[g, half, 0]
            remote(block, block, back_send.at[0], back_recv.at[g, half], right).wait_recv()

    for k in range(count):
        wide[k * chunk : (k + 1) * chunk, :] = returned[k // 4, (k // 2) % 2, k % 2].astype(F32)
    answers[used:slots, :] = jnp.zeros((slots - used, width), BF16)
    for strip in range(strips):
        answers[0:used, strip * LANES : (strip + 1) * LANES] = wide[
            pl.ds(strip, used, stride=strips), :
        ].astype(BF16)
    weights = jnp.concatenate(
        [picks[k : k + LANES, :].T for k in range(0, slots, LANES)], axis=1
    )
    high = weights.astype(BF16)
    low = (weights - high.astype(F32)).astype(BF16)
    for part in range(width // 256):
        columns = slice(part * 256, (part + 1) * 256)
        expert_ref[:, columns] = (
            dot(high, answers[:, columns]) + dot(low, answers[:, columns])
        ).astype(BF16)

    def left_all(amount, sem):
        block = summed.at[pl.ds(0, amount)]
        remote(block, block, sem, z_recv.at[0, 0], right).wait_send()

    left_all(count - 1, z_send.at[0])
    left_all(count - 1, back_send.at[0])
    for side in range(2):
        left_all(count, gather_send.at[side])
        for sem in (relay_send, first_send, direct_send, comb_send):
            left_all(count // 2, sem.at[side])
    for k in range(6):
        block = mix_first.at[0]
        remote(block, block, mix_send.at[k], z_recv.at[0, 0], right).wait_send()


def on_device(
    n_ep,
    n_tp,
    outer_gate,
    inner_gate,
    conv_input,
    conv_taps,
    mixer_weight,
    expert_input,
    norm_gain,
    expert_ids,
    route_weight,
    gate_weight,
    up_weight,
    down_weight,
):
    tokens, width = expert_input.shape
    top = expert_ids.shape[1]
    cap = 5 * tokens * top // (4 * n_ep)
    count = n_ep
    groups = n_ep // CORES // 2
    strips = width // LANES
    chunk = cap * strips
    slots = -(-count * cap // LANES) * LANES
    batch = 4 * 2 * CORES * cap
    length, channels = inner_gate.shape
    units = gate_weight.shape[2]
    vmem, dma = pltpu.VMEM, pltpu.SemaphoreType.DMA
    whole = pl.BlockSpec(memory_space=pltpu.VMEM)
    left_out = pl.BlockSpec(memory_space=pl.ANY)
    block = (groups, 2, CORES, chunk, LANES)
    call = pl.pallas_call(
        functools.partial(kernel, n_ep, n_tp, cap),
        out_shape=[jax.ShapeDtypeStruct((tokens, width), BF16)] * 2,
        in_specs=[whole] * 5 + [left_out] * 7,
        out_specs=[whole] * 2,
        scratch_shapes=[
            vmem((length, channels), BF16),
            vmem((length, channels), BF16),
            vmem((length, channels), BF16),
            vmem((channels, width), BF16),
            vmem((width, units), BF16),
            vmem((width, units), BF16),
            vmem((units, width), BF16),
            vmem((tokens, width), BF16),
            vmem((slots, tokens), F32),
            vmem((count * chunk, LANES), F32),
            vmem((count, chunk, LANES), BF16),
            vmem((groups, 4, 2, CORES, chunk, LANES), BF16),
            vmem((batch * strips, LANES), F32),
            vmem((batch, width), BF16),
            vmem((batch, units), BF16),
            vmem((groups, 4, 2, CORES, chunk, LANES), BF16),
            vmem(block, BF16),
            vmem((groups, 2, 2, CORES, chunk, LANES), BF16),
            vmem(block, BF16),
            vmem((count, chunk, LANES), BF16),
            vmem(block, BF16),
            vmem((slots, width), BF16),
            vmem((8, channels), F32),
            vmem((8, channels), F32),
            vmem((length + 8, channels), F32),
            vmem((4, 2, tokens // 2, width), BF16),
            vmem((2, tokens // 2, width), BF16),
            vmem((2, 2, tokens // 2, width), BF16),
            vmem((2, tokens // 2, width), BF16),
            dma((7,)),
            dma((1,)),
            dma((1,)),
            dma((1,)),
            dma((groups, 2)),
            dma((2,)),
            dma((groups, 2)),
            dma((2,)),
            dma((groups, 2)),
            dma((2,)),
            dma((groups, 2)),
            dma((2,)),
            dma((2,)),
            dma((groups, 2)),
            dma((1,)),
            dma((groups, 2)),
            dma((6,)),
            dma((2,)),
            dma((2, 2)),
        ],
        compiler_params=pltpu.CompilerParams(
            collective_id=0, has_side_effects=True, vmem_limit_bytes=60 * 1024 * 1024
        ),
        name="whole_step",
    )
    mixer_output, expert_output = call(
        expert_ids.T,
        route_weight.T,
        expert_input,
        norm_gain.reshape(1, width),
        conv_taps,
        outer_gate,
        inner_gate,
        conv_input,
        mixer_weight,
        gate_weight[0],
        up_weight[0],
        down_weight[0],
    )
    return mixer_output, expert_output


def solution(mesh):
    rows = P(("grp", "ep", "tp"), None)
    channels = P(("grp", "ep"), "tp")
    return jax.shard_map(
        functools.partial(on_device, mesh.shape["ep"], mesh.shape["tp"]),
        mesh=mesh,
        in_specs=(
            channels,
            channels,
            channels,
            P(None, "tp"),
            P("tp", None),
            rows,
            P(),
            rows,
            rows,
            P("ep", None, "tp"),
            P("ep", None, "tp"),
            P("ep", "tp", None),
        ),
        out_specs=(rows, rows),
        check_vma=False,
    )
```

time: 412 us -> 207 us (0.50); the launches traced: 406 us -> 207 us
  Pallas kernels: 0 us -> 203 us
  waiting for transfers between devices: 196 us -> 0 us
  blocking collectives: 94.4 us -> 0 us
  local copies, waits for them, and re-layouts: 40.7 us -> 3.76 us
  starting transfers between devices: 25.3 us -> 0 us
  matrix products: 20.2 us -> 0 us
  other arithmetic: 15.8 us -> 0 us
  between operations: 14.3 us -> 0.64 us
    pallas_call x0 -> x1, Pallas kernels: none -> 203 us  [on_device(): call(expert_ids.T, route_weight.T, expert_input, norm_gain.reshape(1, wid...]
    all_to_all x3 -> x0, waiting for transfers between devices: 131 us -> none  [the longest x2 74.7 us: summed_on_arrival(): lax.all_to_all(tiles, axis, split_axis=0, concat_axis=0, tiled=True)]
    all_to_all x3 -> x0, blocking collectives: 94.4 us -> none  [exchange_in_order(): lax.all_to_all(tiles, axes[k], split_axis=k, concat_axis=k, tiled=True)]
    all_gather x1 -> x0, waiting for transfers between devices: 64.2 us -> none  [on_device(): block_rows = lax.all_gather(stacked, 'tp', axis=0, tiled=True)]
    all_to_all x3 -> x0, starting transfers between devices: 21.3 us -> none  [the longest x1 12.1 us: exchange_in_order(): lax.all_to_all(tiles, axes[k], split_axis=k, concat_axis=k, tiled=True)]
    dot_general x4 -> x0, matrix products: 20.2 us -> none  [the longest x1 7.24 us: on_device(): jnp.dot(block_rows, gate_local, preferred_element_type=jnp.float32)]
    another operation x7 -> x0, local copies, waits for them, and re-layouts: 13.6 us -> none  [the longest x4 8.68 us: exchange_in_order(): tiles = tiles.reshape(*lengths, *tiles.shape[1:])]
    reduce_sum x5 -> x0, other arithmetic: 13.2 us -> none  [the longest x2 6.29 us: summed_on_arrival(): return arrived.astype(jnp.float32).sum(axis=0)]
  transfers between devices with their start and end apart: 5 -> 0, of which waited for: 5 -> 0; matrix products, arithmetic and copies ran while one was open for 2% -> 0% of each run, Pallas kernels for 0% -> 0%
where the time goes in v1:
time: 207 us
  Pallas kernels  203 us (98%)
  local copies, waits for them, and re-layouts  3.76 us (2%)
    pallas_call x1, Pallas kernels, on_device(): call(expert_ids.T, route_weight.T, expert_input, norm_gain.reshape(1, wid...  203 us

profile of v1, /device:TPU:33, one launch (start us, length us, event | category | flops | bytes accessed | tf_op | source)
XLA Modules:
  0.0 207.2 jit_solution(6880903485850648938)
XLA Ops:
  0.6 202.8 %whole_step.1 = (bf16[128,2048]{1,0:T(8,128)(2,1)}, bf16[128,2048]{1,0:T(8,128)(2,1)}) custom-call(s32[2,128]{1,0:T(2,128)} %bitcast.10, f32[2,128]{1,0:T(2,128)} %bitcast.11, bf16[128,2048]{1,0:T(8,128)(2,1)} %tokens_ref.1, f32[1,2048]{1,0:T(1,128)} %bitcast.9, f32[3,256]{1,0:T(4,128)} %taps_ref.1, bf16[512,256]{1,0:T(8,128)(2,1)} %outer_hbm.1, ...), custom_call_target="tpu_custom_call" | custom-call | tf_op jit(solution)/shard_map/whole_step/pallas_call | solution.py:581
  203.5 1.9 copy.16
  205.4 1.9 copy.17

commit v2 on v1

--- a/solution.py
+++ b/solution.py
@@ -12,8 +12,22 @@
 LANES = 128
 EPSILON = 1e-06
 MESH = pl.DeviceIdType.MESH
+AHEAD = 2
+MIX_AT = 1
 F32 = jnp.float32
 BF16 = jnp.bfloat16
+
+
+def distances(n_z):
+    far = n_z // 2
+    rising = [d for d in range(4, far + 1) if d % 2 == far % 2]
+    falling = [d for d in range(far, 1, -1) if d not in rising]
+    return [1] + rising + falling
+
+
+def offsets(n_z, g):
+    d = distances(n_z)[g]
+    return d, (n_z - d if d < n_z // 2 else 0)
 
 
 def remote(source, target, send, recv, where):
@@ -100,7 +114,7 @@
 ):
     n_z = n_ep // CORES
     groups = n_z // 2
-    last = groups - 1
+    own = distances(n_z).index(groups)
     count = 2 * n_z
     tokens, width = tokens_ref.shape
     strips = width // LANES
@@ -145,15 +159,14 @@
         load.start()
 
     row = lax.broadcasted_iota(jnp.int32, (slots, tokens), 0)
-    place = row * 0
-    for k in range(1, slots // cap + 1):
-        place = place + (row >= k * cap).astype(jnp.int32)
+    place = ((row.astype(F32) + 0.5) * (1.0 / cap)).astype(jnp.int32)
     slot = row - place * cap
     group_of = lax.shift_right_logical(place, 2)
     half_of = lax.shift_right_logical(place, 1) & 1
-    offset = jnp.where(
-        half_of == 0, group_of + 1, jnp.where(group_of == last, 0, n_z - 1 - group_of)
-    )
+    offset = row * 0
+    for g in range(groups):
+        one, two = offsets(n_z, g)
+        offset = jnp.where(group_of == g, jnp.where(half_of == 0, one, two), offset)
     target_z = z - offset
     target_z = jnp.where(target_z < 0, target_z + n_z, target_z)
     expert = jnp.where(row < used, target_z * CORES + (place & 1), -1)
@@ -191,38 +204,26 @@
 
     pl.semaphore_wait(barrier, n_ep + 1)
 
-    def sent(g, half, to_core, from_slot):
-        offset = g + 1 if half == 0 else n_z - 1 - g
-        return remote(
-            outgoing.at[from_slot],
-            gathered.at[g, 0, half, core],
-            z_send.at[0],
-            z_recv.at[g, half],
-            {"ep": ((z + n_z - offset) % n_z) * CORES + to_core},
-        )
-
-    @pl.loop(0, last)
-    def _(g):
-        for half in range(2):
-            for to_core in range(CORES):
-                sent(g, half, to_core, 4 * g + 2 * half + to_core).start()
-
-    for to_core in range(CORES):
-        sent(last, 0, to_core, 4 * last + to_core).start()
     other = 1 - core
-    partner = {"ep": z * CORES + other}
-    remote(
-        outgoing.at[4 * last + 2 + other],
-        gathered.at[last, 0, 1, core],
-        z_send.at[0],
-        z_recv.at[last, 1],
-        partner,
-    ).start()
-    gathered[last, 0, 1, core] = outgoing[4 * last + 2 + core]
+
+    def z_send_group(g):
+        for half, offset in enumerate(offsets(n_z, g)):
+            for to_core in range(CORES) if offset else (other,):
+                remote(
+                    outgoing.at[4 * g + 2 * half + to_core],
+                    gathered.at[g, 0, half, core],
+                    z_send.at[0],
+                    z_recv.at[g, half],
+                    {"ep": ((z + n_z - offset) % n_z) * CORES + to_core},
+                ).start()
+
     halo = remote(
         tail_out, tail_in, halo_send.at[0], halo_recv.at[0], {"ep": (me + 1) % n_ep}
     )
     halo.start()
+    for g in range(AHEAD):
+        z_send_group(g)
+    gathered[own, 0, 1, core] = outgoing[4 * own + 2 + core]
 
     for load in loads[2:4]:
         load.wait()
@@ -252,15 +253,21 @@
         block = gathered.at[g, 0, 0]
         remote(block, block, z_send.at[0], z_recv.at[g, 0], right).wait_recv()
 
-        @pl.when(g < last)
+        @pl.when(g != own)
         def _():
             block = gathered.at[g, 0, 1]
             remote(block, block, z_send.at[0], z_recv.at[g, 1], right).wait_recv()
 
-        @pl.when(g == last)
+        @pl.when(g == own)
         def _():
             block = gathered.at[g, 0, 1, 0]
             remote(block, block, z_send.at[0], z_recv.at[g, 1], right).wait_recv()
+
+        for k in range(AHEAD, groups):
+
+            @pl.when(g == k - AHEAD)
+            def _():
+                z_send_group(k)
 
         remote(
             gathered.at[g, 0], gathered.at[g, 3], gather_send.at[0], gather_recv.at[g, 0], right
@@ -340,16 +347,6 @@
                 second_recv.at[g, side], where,
             ).start()
 
-    def back(g, half, to_core):
-        offset = g + 1 if half == 0 else n_z - 1 - g
-        return remote(
-            summed.at[4 * g + 2 * half + to_core],
-            returned.at[g, half, core],
-            back_send.at[0],
-            back_recv.at[g, half],
-            {"ep": ((z + offset) % n_z) * CORES + to_core},
-        )
-
     def give_back(g):
         for side, where in ((0, right), (1, left)):
             block = second_in.at[g, side]
@@ -362,24 +359,23 @@
                     + second_in[g, 1, half, from_core].astype(F32)
                 ).astype(BF16)
 
-        @pl.when(g < last)
-        def _():
-            for half in range(2):
-                for to_core in range(CORES):
-                    back(g, half, to_core).start()
-
-        @pl.when(g == last)
-        def _():
-            for to_core in range(CORES):
-                back(last, 0, to_core).start()
-            remote(
-                summed.at[4 * last + 2 + other],
-                returned.at[last, 1, core],
-                back_send.at[0],
-                back_recv.at[last, 1],
-                partner,
-            ).start()
-            returned[last, 1, core] = summed[4 * last + 2 + core]
+        for k in range(groups):
+
+            @pl.when(g == k)
+            def _():
+                for half, offset in enumerate(offsets(n_z, k)):
+                    for to_core in range(CORES) if offset else (other,):
+                        remote(
+                            summed.at[4 * k + 2 * half + to_core],
+                            returned.at[k, half, core],
+                            back_send.at[0],
+                            back_recv.at[k, half],
+                            {"ep": ((z + offset) % n_z) * CORES + to_core},
+                        ).start()
+
+        @pl.when(g == own)
+        def _():
+            returned[own, 1, core] = summed[4 * own + 2 + core]
 
     def mix_start():
         remote(
@@ -409,33 +405,36 @@
                 mix_second_recv.at[side, side], where,
             ).start()
 
-    @pl.loop(0, groups + 4)
+    @pl.loop(0, groups + 2)
     def _(t):
-        @pl.when((t >= 2) & (t < groups + 2))
-        def _():
-            compute(t - 2)
-
-        @pl.when((t >= 3) & (t < groups + 3))
-        def _():
-            combine(t - 3)
-
-        @pl.when(t == groups + 2)
+        @pl.when(t < groups)
+        def _():
+            gather(t)
+
+        @pl.when(t == MIX_AT)
         def _():
             mix_start()
 
-        @pl.when(t >= 4)
-        def _():
-            give_back(t - 4)
+        @pl.when(t == MIX_AT + 1)
+        def _():
+            mix_combine()
 
         @pl.when((t >= 1) & (t < groups + 1))
         def _():
-            relay(t - 1)
+            compute(t - 1)
 
         @pl.when(t < groups)
         def _():
-            gather(t)
-
-    mix_combine()
+            relay(t)
+
+        @pl.when(t >= 2)
+        def _():
+            give_back(t - 2)
+
+        @pl.when((t >= 1) & (t < groups + 1))
+        def _():
+            combine(t - 1)
+
     for side in range(2):
         for half in range(2):
             block = mix_second.at[side, half]
@@ -451,7 +450,7 @@
 
     for g in range(groups):
         for half in range(2):
-            block = returned.at[g, half] if (g, half) != (last, 1) else returned.at[g, half, 0]
+            block = returned.at[g, half] if (g, half) != (own, 1) else returned.at[g, half, 0]
             remote(block, block, back_send.at[0], back_recv.at[g, half], right).wait_recv()
 
     for k in range(count):

time: 207 us -> 160 us (0.77)
  Pallas kernels: 203 us -> 155 us
    pallas_call x1, Pallas kernels: 203 us -> 155 us  [on_device(): call(expert_ids.T, route_weight.T, expert_input, norm_gain.reshape(1, wid...]
where the time goes in v2:
time: 160 us
  Pallas kernels  155 us (97%)
  local copies, waits for them, and re-layouts  3.76 us (2%)
    pallas_call x1, Pallas kernels, on_device(): call(expert_ids.T, route_weight.T, expert_input, norm_gain.reshape(1, wid...  155 us
    unnamed x2, local copies, waits for them, and re-layouts  3.76 us

profile of v2, /device:TPU:33, one launch (start us, length us, event | category | flops | bytes accessed | tf_op | source)
XLA Modules:
  0.0 159.8 jit_solution(14654044412016272332)
XLA Ops:
  0.6 155.4 %whole_step.1 = (bf16[128,2048]{1,0:T(8,128)(2,1)}, bf16[128,2048]{1,0:T(8,128)(2,1)}) custom-call(s32[2,128]{1,0:T(2,128)} %bitcast.10, f32[2,128]{1,0:T(2,128)} %bitcast.11, bf16[128,2048]{1,0:T(8,128)(2,1)} %tokens_ref.1, f32[1,2048]{1,0:T(1,128)} %bitcast.9, f32[3,256]{1,0:T(4,128)} %taps_ref.1, bf16[512,256]{1,0:T(8,128)(2,1)} %outer_hbm.1, ...), custom_call_target="tpu_custom_call" | custom-call | tf_op jit(solution)/shard_map/whole_step/pallas_call | solution.py:580
  156.0 1.9 %copy.16 = bf16[128,2048]{1,0:T(8,128)(2,1)} copy(bf16[128,2048]{1,0:T(8,128)(2,1)} %get-tuple-element.4) | data formatting | bytes 1048576
  157.9 1.9 %copy.17 = bf16[128,2048]{1,0:T(8,128)(2,1)} copy(bf16[128,2048]{1,0:T(8,128)(2,1)} %get-tuple-element.5) | data formatting | bytes 1048576

commit v3 on v2

--- a/solution.py
+++ b/solution.py
@@ -12,8 +12,10 @@
 LANES = 128
 EPSILON = 1e-06
 MESH = pl.DeviceIdType.MESH
-AHEAD = 2
-MIX_AT = 1
+AHEAD = 3
+FIRST = 2
+GRANT = 58
+PIECES = 4
 F32 = jnp.float32
 BF16 = jnp.bfloat16
 
@@ -49,11 +51,11 @@
     n_ep,
     n_tp,
     cap,
-    ids_ref,
-    route_ref,
-    tokens_ref,
-    gain_ref,
-    taps_ref,
+    ids_hbm,
+    route_hbm,
+    tokens_hbm,
+    gain_hbm,
+    taps_hbm,
     outer_hbm,
     inner_hbm,
     conv_hbm,
@@ -63,6 +65,11 @@
     down_hbm,
     mixer_ref,
     expert_ref,
+    ids_ref,
+    route_ref,
+    tokens_ref,
+    gain_ref,
+    taps_ref,
     outer,
     inner,
     conv,
@@ -92,6 +99,8 @@
     mix_first,
     mix_second,
     mix_combined,
+    total,
+    small_sem,
     load_sem,
     halo_send,
     halo_recv,
@@ -141,6 +150,20 @@
     pl.semaphore_signal(barrier, inc=1, device_id=right, device_id_type=MESH)
     pl.semaphore_signal(barrier, inc=1, device_id=left, device_id_type=MESH)
 
+    smalls = [
+        pltpu.make_async_copy(source, target, small_sem.at[k])
+        for k, (source, target) in enumerate(
+            (
+                (ids_hbm, ids_ref),
+                (route_hbm, route_ref),
+                (tokens_hbm, tokens_ref),
+                (gain_hbm, gain_ref),
+                (taps_hbm, taps_ref),
+            )
+        )
+    ]
+    for small in smalls:
+        small.start()
     loads = [
         pltpu.make_async_copy(source, target, load_sem.at[k])
         for k, (source, target) in enumerate(
@@ -157,6 +180,9 @@
     ]
     for load in loads:
         load.start()
+
+    smalls[0].wait()
+    smalls[1].wait()
 
     row = lax.broadcasted_iota(jnp.int32, (slots, tokens), 0)
     place = ((row.astype(F32) + 0.5) * (1.0 / cap)).astype(jnp.int32)
@@ -183,6 +209,8 @@
     )
     picks[...] = chosen * weight
 
+    for small in smalls[2:]:
+        small.wait()
     values = tokens_ref[...].astype(F32)
     mean = jnp.mean(values * values, axis=1, keepdims=True)
     normed[...] = (values * lax.rsqrt(mean + EPSILON) * gain_ref[...]).astype(BF16)
@@ -221,7 +249,7 @@
         tail_out, tail_in, halo_send.at[0], halo_recv.at[0], {"ep": (me + 1) % n_ep}
     )
     halo.start()
-    for g in range(AHEAD):
+    for g in range(FIRST):
         z_send_group(g)
     gathered[own, 0, 1, core] = outgoing[4 * own + 2 + core]
 
@@ -246,6 +274,8 @@
             columns = slice(part * 512, (part + 1) * 512)
             mix_partial[k // 2, k % 2, :, columns] = dot(mixed, mixw[:, columns]).astype(BF16)
 
+    for g in range(FIRST, min(AHEAD, groups)):
+        z_send_group(g)
     for load in loads[4:]:
         load.wait()
 
@@ -405,35 +435,54 @@
                 mix_second_recv.at[side, side], where,
             ).start()
 
+    mix_start()
+
     @pl.loop(0, groups + 2)
     def _(t):
         @pl.when(t < groups)
         def _():
             gather(t)
 
-        @pl.when(t == MIX_AT)
-        def _():
-            mix_start()
-
-        @pl.when(t == MIX_AT + 1)
+        @pl.when((t >= 1) & (t < groups + 1))
+        def _():
+            compute(t - 1)
+
+        @pl.when(t < groups)
+        def _():
+            relay(t)
+
+        @pl.when(t >= 2)
+        def _():
+            give_back(t - 2)
+
+        @pl.when((t >= 1) & (t < groups + 1))
+        def _():
+            combine(t - 1)
+
+        @pl.when(t == groups - 1)
         def _():
             mix_combine()
 
-        @pl.when((t >= 1) & (t < groups + 1))
-        def _():
-            compute(t - 1)
-
-        @pl.when(t < groups)
-        def _():
-            relay(t)
-
-        @pl.when(t >= 2)
-        def _():
-            give_back(t - 2)
-
-        @pl.when((t >= 1) & (t < groups + 1))
-        def _():
-            combine(t - 1)
+    weights = jnp.concatenate(
+        [picks[k : k + LANES, :].T for k in range(0, slots, LANES)], axis=1
+    )
+    high = weights.astype(BF16)
+    low = (weights - high.astype(F32)).astype(BF16)
+    answers[used:slots, :] = jnp.zeros((slots - used, width), BF16)
+
+    def arrived(begin, end):
+        for g in range(begin, end):
+            for half in range(2):
+                block = returned.at[g, half] if (g, half) != (own, 1) else returned.at[g, half, 0]
+                remote(block, block, back_send.at[0], back_recv.at[g, half], right).wait_recv()
+        start = 4 * begin * cap
+        rows = 4 * (end - begin) * cap
+        for k in range(4 * begin, 4 * end):
+            wide[k * chunk : (k + 1) * chunk, :] = returned[k // 4, (k // 2) % 2, k % 2].astype(F32)
+        for strip in range(strips):
+            answers[start : start + rows, strip * LANES : (strip + 1) * LANES] = wide[
+                pl.ds(start * strips + strip, rows, stride=strips), :
+            ].astype(BF16)
 
     for side in range(2):
         for half in range(2):
@@ -447,28 +496,18 @@
             + mix_second[0, half].astype(F32)
             + mix_second[1, half].astype(F32)
         ).astype(BF16)
-
-    for g in range(groups):
-        for half in range(2):
-            block = returned.at[g, half] if (g, half) != (own, 1) else returned.at[g, half, 0]
-            remote(block, block, back_send.at[0], back_recv.at[g, half], right).wait_recv()
-
-    for k in range(count):
-        wide[k * chunk : (k + 1) * chunk, :] = returned[k // 4, (k // 2) % 2, k % 2].astype(F32)
-    answers[used:slots, :] = jnp.zeros((slots - used, width), BF16)
-    for strip in range(strips):
-        answers[0:used, strip * LANES : (strip + 1) * LANES] = wide[
-            pl.ds(strip, used, stride=strips), :
-        ].astype(BF16)
-    weights = jnp.concatenate(
-        [picks[k : k + LANES, :].T for k in range(0, slots, LANES)], axis=1
-    )
-    high = weights.astype(BF16)
-    low = (weights - high.astype(F32)).astype(BF16)
+    arrived(0, groups - 1)
+    done = 4 * (groups - 1) * cap // LANES * LANES
     for part in range(width // 256):
         columns = slice(part * 256, (part + 1) * 256)
+        rows = answers[0:done, columns]
+        total[:, columns] = dot(high[:, 0:done], rows) + dot(low[:, 0:done], rows)
+    arrived(groups - 1, groups)
+    for part in range(width // 256):
+        columns = slice(part * 256, (part + 1) * 256)
+        rows = answers[done:slots, columns]
         expert_ref[:, columns] = (
-            dot(high, answers[:, columns]) + dot(low, answers[:, columns])
+            total[:, columns] + dot(high[:, done:slots], rows) + dot(low[:, done:slots], rows)
         ).astype(BF16)
 
     def left_all(amount, sem):
@@ -484,6 +523,28 @@
     for k in range(6):
         block = mix_first.at[0]
         remote(block, block, mix_send.at[k], z_recv.at[0, 0], right).wait_send()
+
+
+def hand_on(one, two, one_out, two_out, held, in_sem, out_sem):
+    rows = one.shape[0] // PIECES
+    steps = []
+    for k, (source, target) in enumerate(((one, one_out), (two, two_out))):
+        for piece in range(PIECES):
+            where = pl.ds(piece * rows, rows)
+            place = held.at[k, where]
+            steps.append(
+                (
+                    pltpu.make_async_copy(source.at[where], place, in_sem.at[k, piece]),
+                    pltpu.make_async_copy(place, target.at[where], out_sem.at[k, piece]),
+                )
+            )
+    for arrive, _ in steps:
+        arrive.start()
+    for arrive, leave in steps:
+        arrive.wait()
+        leave.start()
+    for _, leave in steps:
+        leave.wait()
 
 
 def on_device(
@@ -515,14 +576,19 @@
     units = gate_weight.shape[2]
     vmem, dma = pltpu.VMEM, pltpu.SemaphoreType.DMA
     whole = pl.BlockSpec(memory_space=pltpu.VMEM)
-    left_out = pl.BlockSpec(memory_space=pl.ANY)
+    left_out = pl.BlockSpec(memory_space=pltpu.HBM)
     block = (groups, 2, CORES, chunk, LANES)
     call = pl.pallas_call(
         functools.partial(kernel, n_ep, n_tp, cap),
         out_shape=[jax.ShapeDtypeStruct((tokens, width), BF16)] * 2,
-        in_specs=[whole] * 5 + [left_out] * 7,
+        in_specs=[left_out] * 12,
         out_specs=[whole] * 2,
         scratch_shapes=[
+            vmem((top, tokens), jnp.int32),
+            vmem((top, tokens), F32),
+            vmem((tokens, width), BF16),
+            vmem((1, width), F32),
+            vmem((TAPS, channels), F32),
             vmem((length, channels), BF16),
             vmem((length, channels), BF16),
             vmem((length, channels), BF16),
@@ -552,6 +618,8 @@
             vmem((2, tokens // 2, width), BF16),
             vmem((2, 2, tokens // 2, width), BF16),
             vmem((2, tokens // 2, width), BF16),
+            vmem((tokens, width), F32),
+            dma((5,)),
             dma((7,)),
             dma((1,)),
             dma((1,)),
@@ -573,7 +641,7 @@
             dma((2, 2)),
         ],
         compiler_params=pltpu.CompilerParams(
-            collective_id=0, has_side_effects=True, vmem_limit_bytes=60 * 1024 * 1024
+            collective_id=0, has_side_effects=True, vmem_limit_bytes=GRANT * 1024 * 1024
         ),
         name="whole_step",
     )
@@ -591,7 +659,19 @@
         up_weight[0],
         down_weight[0],
     )
-    return mixer_output, expert_output
+    return pl.pallas_call(
+        hand_on,
+        out_shape=[jax.ShapeDtypeStruct((tokens, width), BF16)] * 2,
+        in_specs=[left_out] * 2,
+        out_specs=[left_out] * 2,
+        scratch_shapes=[
+            vmem((2, tokens, width), BF16),
+            dma((2, PIECES)),
+            dma((2, PIECES)),
+        ],
+        compiler_params=pltpu.CompilerParams(vmem_limit_bytes=GRANT * 1024 * 1024),
+        name="hand_on",
+    )(mixer_output, expert_output)
 
 
 def solution(mesh):

time: 160 us -> 152 us (0.950)
  Pallas kernels: 155 us -> 151 us
  local copies, waits for them, and re-layouts: 3.76 us -> 0 us
    pallas_call x1, Pallas kernels: 155 us -> 149 us  [on_device(): call(expert_ids.T, route_weight.T, expert_input, norm_gain.reshape(1, wid...]
    unnamed x2 -> x0, local copies, waits for them, and re-layouts: 3.76 us -> none
    pallas_call x0 -> x1, Pallas kernels: none -> 2.09 us  [on_device(): pl.pallas_call(hand_on, out_shape=[jax.ShapeDtypeStruct((tokens, width),...]
where the time goes in v3:
time: 152 us
  Pallas kernels  151 us (99%)
    pallas_call x1, Pallas kernels, on_device(): call(expert_ids.T, route_weight.T, expert_input, norm_gain.reshape(1, wid...  149 us

profile of v3, /device:TPU:33, one launch (start us, length us, event | category | flops | bytes accessed | tf_op | source)
XLA Modules:
  0.0 151.9 jit_solution(2708144010886644180)
XLA Ops:
  0.6 149.2 %whole_step.1 = (bf16[128,2048]{1,0:T(8,128)(2,1)}, bf16[128,2048]{1,0:T(8,128)(2,1)}) custom-call(s32[2,128]{1,0:T(2,128)} %bitcast.10, f32[2,128]{1,0:T(2,128)} %bitcast.11, bf16[128,2048]{1,0:T(8,128)(2,1)} %tokens_hbm.1, f32[1,2048]{1,0:T(1,128)} %bitcast.9, f32[3,256]{1,0:T(4,128)} %taps_hbm.1, bf16[512,256]{1,0:T(8,128)(2,1)} %outer_hbm.1, ...), custom_call_target="tpu_custom_call" | custom-call | tf_op jit(solution)/shard_map/whole_step/pallas_call | solution.py:648
  149.8 2.1 %hand_on.1 = (bf16[128,2048]{1,0:T(8,128)(2,1)}, bf16[128,2048]{1,0:T(8,128)(2,1)}) custom-call(bf16[128,2048]{1,0:T(8,128)(2,1)} %get-tuple-element.4.one, bf16[128,2048]{1,0:T(8,128)(2,1)} %get-tuple-element.5.two), custom_call_target="tpu_custom_call" | custom-call | tf_op jit(solution)/shard_map/hand_on/pallas_call | solution.py:662

commit v4 on v3

--- a/solution.py
+++ b/solution.py
@@ -13,7 +13,7 @@
 EPSILON = 1e-06
 MESH = pl.DeviceIdType.MESH
 AHEAD = 3
-FIRST = 2
+FIRST = 1
 GRANT = 58
 PIECES = 4
 F32 = jnp.float32
@@ -21,10 +21,7 @@
 
 
 def distances(n_z):
-    far = n_z // 2
-    rising = [d for d in range(4, far + 1) if d % 2 == far % 2]
-    falling = [d for d in range(far, 1, -1) if d not in rising]
-    return [1] + rising + falling
+    return [1] + list(range(n_z // 2, 1, -1))
 
 
 def offsets(n_z, g):

time: 152 us -> 151 us (level)
  no operation moved by 1% of the time
where the time goes in v4:
time: 151 us
  Pallas kernels  150 us (99%)
    pallas_call x1, Pallas kernels, on_device(): call(expert_ids.T, route_weight.T, expert_input, norm_gain.reshape(1, wid...  148 us

profile of v4, /device:TPU:33, one launch (start us, length us, event | category | flops | bytes accessed | tf_op | source)
XLA Modules:
  0.0 150.8 jit_solution(2742375390701180703)
XLA Ops:
  0.6 148.1 %whole_step.1 = (bf16[128,2048]{1,0:T(8,128)(2,1)}, bf16[128,2048]{1,0:T(8,128)(2,1)}) custom-call(s32[2,128]{1,0:T(2,128)} %bitcast.10, f32[2,128]{1,0:T(2,128)} %bitcast.11, bf16[128,2048]{1,0:T(8,128)(2,1)} %tokens_hbm.1, f32[1,2048]{1,0:T(1,128)} %bitcast.9, f32[3,256]{1,0:T(4,128)} %taps_hbm.1, bf16[512,256]{1,0:T(8,128)(2,1)} %outer_hbm.1, ...), custom_call_target="tpu_custom_call" | custom-call | tf_op jit(solution)/shard_map/whole_step/pallas_call | solution.py:645
  148.7 2.1 %hand_on.1 = (bf16[128,2048]{1,0:T(8,128)(2,1)}, bf16[128,2048]{1,0:T(8,128)(2,1)}) custom-call(bf16[128,2048]{1,0:T(8,128)(2,1)} %get-tuple-element.4.one, bf16[128,2048]{1,0:T(8,128)(2,1)} %get-tuple-element.5.two), custom_call_target="tpu_custom_call" | custom-call | tf_op jit(solution)/shard_map/hand_on/pallas_call | solution.py:659
